TPU v7x, 32 devices: a whole 2x2x4 slice. The times are simulated.
32 devices in a mesh: pp: 4 (over z), fs: 4 (over y, x), tp: 2 (over core).
Axes of the slice: x: 2, y: 2, z: 4, core: 2. Of those that a mesh axis runs over, the one named last changes fastest.
Arguments:
- tokens: bfloat16 [4, 8, 128, 2048], P('pp', ('fs', 'tp')), may hold values from -6 to 6
- layer_norm_scale: float32 [4, 2048], P('pp'), may hold values from 0.1 to 1.9
- input_weight: bfloat16 [4, 2048, 1024], P('pp'), may hold values from -0.125 to 0.125
- filter_weight: float32 [4, 4, 1024], P('pp'), may hold values from -3 to 3
- filter_bias: float32 [4, 1024], P('pp'), may hold values from -2 to 2
- recur_gate_weight: bfloat16 [4, 8, 128, 128], P('pp'), may hold values from -0.5 to 0.5
- recur_gate_bias: float32 [4, 1024], P('pp'), may hold values from -4 to 4
- input_gate_weight: bfloat16 [4, 8, 128, 128], P('pp'), may hold values from -0.5 to 0.5
- input_gate_bias: float32 [4, 1024], P('pp'), may hold values from -4 to 4
- decay_setting: float32 [4, 1024], P('pp'), may hold values from -2 to 8
- spike_log_decay: float32 [4, 128], P('pp'), may hold values from -0.7 to 0, as said below
- output_weight: bfloat16 [4, 1024, 2048], P('pp'), may hold values from -0.375 to 0.375
Outputs:
- result: bfloat16 [4, 8, 128, 2048], P('pp', ('fs', 'tp'))
Inputs may be any that keep to these rules, and one draw needn't show every extreme that they name: `spike_log_decay`: zero at most positions; at a few positions of each layer drawn from the seed it lies between log(0.5) and log(0.8).
All inputs are finite; a program needn't handle non-finite values.
Results may differ from a plain program's by a relative error of at most 0.023.
Values may be sent and summed in bfloat16 or wider, within the bound.
A program may use at most 64 MiB of HBM per device.

v0:
```python
import jax
import jax.numpy as jnp
from jax import lax
from jax.sharding import PartitionSpec as P


def from_behind(value, axis, by):
    devices = lax.axis_size(axis)
    return lax.ppermute(value, axis, [(i, (i + by) % devices) for i in range(devices)])


def combine_pair(left, right):
    return (left[0] * right[0], right[0] * left[1] + right[1])


def one_layer(hidden, weight_bundle):
    (
        norm_factor,
        input_projected,
        filter_kernel_taps,
        filter_offset,
        retention_weight,
        retention_bias,
        injection_weight,
        injection_bias,
        unscaled_decay,
        decay_spike,
        output_projected,
    ) = weight_bundle
    width = input_projected.shape[1]
    taps = filter_kernel_taps.shape[0]
    blocks = retention_weight.shape[0]
    length = hidden.shape[0]
    hidden32 = hidden.astype(jnp.float32)
    squares = jnp.mean(hidden32 * hidden32, axis=-1, keepdims=True)
    normed = (hidden32 * lax.rsqrt(squares + 1e-06) * norm_factor).astype(jnp.bfloat16)
    mixed_in = jnp.dot(normed, input_projected, preferred_element_type=jnp.float32).astype(
        jnp.bfloat16
    )
    padded = jnp.pad(mixed_in.astype(jnp.float32), ((taps - 1, 0), (0, 0)))
    conv_out = filter_offset + sum(
        (padded[k : k + length] * filter_kernel_taps[k] for k in range(taps))
    )
    conv_out = conv_out.astype(jnp.bfloat16)
    grouped = conv_out.reshape(length, blocks, -1)
    retention_gate = jax.nn.sigmoid(
        jnp.einsum(
            "ngi,gij->ngj", grouped, retention_weight, preferred_element_type=jnp.float32
        ).reshape(length, width)
        + retention_bias
    )
    inject = jax.nn.sigmoid(
        jnp.einsum(
            "ngi,gij->ngj", grouped, injection_weight, preferred_element_type=jnp.float32
        ).reshape(length, width)
        + injection_bias
    )
    decay_logarithm = (
        -8.0 * retention_gate * jax.nn.softplus(-unscaled_decay) + decay_spike[:, None]
    )
    decay = jnp.exp(decay_logarithm)
    update = jnp.sqrt(-jnp.expm1(2.0 * decay_logarithm)) * inject * conv_out.astype(jnp.float32)
    states = lax.associative_scan(combine_pair, (decay, update), axis=0)[1].astype(jnp.bfloat16)
    projected = jnp.dot(states, output_projected, preferred_element_type=jnp.float32)
    return (hidden32 + projected).astype(jnp.bfloat16)


def local(
    tokens,
    layer_norm_scale,
    input_weight,
    filter_weight,
    filter_bias,
    recur_gate_weight,
    recur_gate_bias,
    input_gate_weight,
    input_gate_bias,
    decay_setting,
    spike_log_decay,
    output_weight,
):
    sections = lax.axis_size("pp")
    section_id = lax.axis_index("pp")
    weight_bundle = (
        layer_norm_scale[0],
        input_weight[0],
        filter_weight[0],
        filter_bias[0],
        recur_gate_weight[0],
        recur_gate_bias[0],
        input_gate_weight[0],
        input_gate_bias[0],
        decay_setting[0],
        spike_log_decay[0],
        output_weight[0],
    )
    initial = tokens[0, 0]

    def run_layer(activations):
        return one_layer(activations, weight_bundle)

    def passed(activations):
        return activations

    def advance(moment, carried):
        active = (moment >= section_id) & (moment < section_id + sections)
        layered = lax.cond(active, run_layer, passed, carried)
        return from_behind(layered, "pp", 1)

    finished = lax.fori_loop(0, 2 * sections, advance, initial)
    return finished[None, None]


def solution(mesh):
    placed = (
        P("pp", ("fs", "tp"), None, None),
        P("pp", None),
        P("pp", None, None),
        P("pp", None, None),
        P("pp", None),
        P("pp", None, None, None),
        P("pp", None),
        P("pp", None, None, None),
        P("pp", None),
        P("pp", None),
        P("pp", None),
        P("pp", None, None),
    )
    return jax.shard_map(
        local,
        mesh=mesh,
        in_specs=placed,
        out_specs=P("pp", ("fs", "tp"), None, None),
        check_vma=False,
    )
```

profile of v0, /device:TPU:0, one launch (start us, length us, event | category | flops | bytes accessed | tf_op | source)
XLA Modules:
  0.0 203.8 jit_solution(2978256510549942267)
XLA Ops:
  0.0 1.0 copy.40
  1.0 1.1 copy.17
  2.2 1.8 copy.18
  4.0 199.0 %while.17 = (s32[]{:T(128)}, bf16[128,2048]{1,0:T(8,128)(2,1)S(1)}, s32[]{:T(128)}, s32[]{:T(128)}, f32[1,1024]{1,0:T(1,128)}, /*index=5*/f32[1,2048]{1,0:T(1,12...) while((s32[]{:T(128)}, bf16[128,2048]{1,0:T(8,128)(2,1)S(1)}, ...), condition=%wide.region_4.5_spmd, body=%wide.region_0.4_spmd.sunk | while | flops 1149344896 | bytes 40322016 | solution.py:110
  4.0 14.1 %conditional.2 = (bf16[128,2048]{1,0:T(8,128)(2,1)S(1)}) conditional(s32[]{:T(128)} %convert_element_type.60, bf16[128,2048]{1,0:T(8,128)(2,1)S(1)} %get-tuple-element.499, (bf16[128,2048]{1,0:T(8,128)(2,1)S(1)}, f32[1,1024]{1,0:T(1,128)}, f32[1,2048]{1,0:T(1,128)}, bf16[2048,1024]{1,0:T(8,128)(2,1)}, f32[4,1024]{1,0:T(4,128)}, ...), branch_computations={%region_1.0_spmd, %region_2.3_spmd} | conditional | flops 1149344896 | bytes 37175976 | solution.py:107
  4.2 0.7 fusion.22
  4.9 0.9 fusion.31
  5.8 3.0 %fusion.1 = f32[128,1024]{1,0:T(8,128)S(1)} fusion(bf16[2048,1024]{1,0:T(8,128)(2,1)} %get-tuple-element.314, bf16[128,2048]{1,0:T(8,128)(2,1)S(1)} %get-tuple-element.311, f32[2048]{0:T(1024)} %bitcast.51, f32[128]{0:T(128)S(1)} %add_rsqrt_fusion), kind=kOutput, calls=%fused_computation.5 | convolution fusion | flops 538181632 | bytes 5251584 | tf_op jit(solution)/shard_map/while/body/eval_jaxpr/cond/branch_1_fun/dot_general | solution.py:37
  9.1 1.3 fusion.9
  10.3 0.3 fusion.11
  11.1 0.8 fusion.24
  15.0 3.1 %fusion = bf16[128,2048]{1,0:T(8,128)(2,1)S(1)} fusion(bf16[1024,2048]{1,0:T(8,128)(2,1)} %get-tuple-element.322, bf16[128,2048]{1,0:T(8,128)(2,1)S(1)} %get-tuple-element.311, f32[128,1024]{1,0:T(8,128)S(1)} %pad.45, f32[128,1024]{1,0:T(8,128)S(1)} %pad.46), kind=kOutput, calls=%fused_computation.1 | convolution fusion | flops 537919488 | bytes 6291456 | tf_op jit(solution)/shard_map/while/body/eval_jaxpr/cond/branch_1_fun/dot_general | solution.py:64
  18.2 16.1 %collective-permute-done = bf16[128,2048]{1,0:T(8,128)(2,1)S(1)} collective-permute-done((bf16[128,2048]{1,0:T(8,128)(2,1)S(1)}, bf16[128,2048]{1,0:T(8,128)(2,1)S(1)}, u32[]{:S(2)}, u32[]{:S(2)}) %collective-permute-start) | collective-permute-done | bytes 524320 | tf_op jit(solution)/shard_map/while/body/eval_jaxpr/ppermute | solution.py:9
  34.3 14.2 %conditional.2 = (bf16[128,2048]{1,0:T(8,128)(2,1)S(1)}) conditional(s32[]{:T(128)} %convert_element_type.60, bf16[128,2048]{1,0:T(8,128)(2,1)S(1)} %get-tuple-element.499, (bf16[128,2048]{1,0:T(8,128)(2,1)S(1)}, f32[1,1024]{1,0:T(1,128)}, f32[1,2048]{1,0:T(1,128)}, bf16[2048,1024]{1,0:T(8,128)(2,1)}, f32[4,1024]{1,0:T(4,128)}, ...), branch_computations={%region_1.0_spmd, %region_2.3_spmd} | conditional | flops 1149344896 | bytes 37175976 | solution.py:107
  34.6 0.7 fusion.22
  35.3 0.9 fusion.31
  36.2 3.0 %fusion.1 = f32[128,1024]{1,0:T(8,128)S(1)} fusion(bf16[2048,1024]{1,0:T(8,128)(2,1)} %get-tuple-element.314, bf16[128,2048]{1,0:T(8,128)(2,1)S(1)} %get-tuple-element.311, f32[2048]{0:T(1024)} %bitcast.51, f32[128]{0:T(128)S(1)} %add_rsqrt_fusion), kind=kOutput, calls=%fused_computation.5 | convolution fusion | flops 538181632 | bytes 5251584 | tf_op jit(solution)/shard_map/while/body/eval_jaxpr/cond/branch_1_fun/dot_general | solution.py:37
  39.5 1.3 fusion.9
  40.7 0.3 fusion.11
  41.5 0.8 fusion.24
  45.4 3.1 %fusion = bf16[128,2048]{1,0:T(8,128)(2,1)S(1)} fusion(bf16[1024,2048]{1,0:T(8,128)(2,1)} %get-tuple-element.322, bf16[128,2048]{1,0:T(8,128)(2,1)S(1)} %get-tuple-element.311, f32[128,1024]{1,0:T(8,128)S(1)} %pad.45, f32[128,1024]{1,0:T(8,128)S(1)} %pad.46), kind=kOutput, calls=%fused_computation.1 | convolution fusion | flops 537919488 | bytes 6291456 | tf_op jit(solution)/shard_map/while/body/eval_jaxpr/cond/branch_1_fun/dot_general | solution.py:64
  48.6 15.2 %collective-permute-done = bf16[128,2048]{1,0:T(8,128)(2,1)S(1)} collective-permute-done((bf16[128,2048]{1,0:T(8,128)(2,1)S(1)}, bf16[128,2048]{1,0:T(8,128)(2,1)S(1)}, u32[]{:S(2)}, u32[]{:S(2)}) %collective-permute-start) | collective-permute-done | bytes 524320 | tf_op jit(solution)/shard_map/while/body/eval_jaxpr/ppermute | solution.py:9
  63.8 14.2 %conditional.2 = (bf16[128,2048]{1,0:T(8,128)(2,1)S(1)}) conditional(s32[]{:T(128)} %convert_element_type.60, bf16[128,2048]{1,0:T(8,128)(2,1)S(1)} %get-tuple-element.499, (bf16[128,2048]{1,0:T(8,128)(2,1)S(1)}, f32[1,1024]{1,0:T(1,128)}, f32[1,2048]{1,0:T(1,128)}, bf16[2048,1024]{1,0:T(8,128)(2,1)}, f32[4,1024]{1,0:T(4,128)}, ...), branch_computations={%region_1.0_spmd, %region_2.3_spmd} | conditional | flops 1149344896 | bytes 37175976 | solution.py:107
  64.1 0.7 fusion.22
  64.8 0.9 fusion.31
  65.7 3.0 %fusion.1 = f32[128,1024]{1,0:T(8,128)S(1)} fusion(bf16[2048,1024]{1,0:T(8,128)(2,1)} %get-tuple-element.314, bf16[128,2048]{1,0:T(8,128)(2,1)S(1)} %get-tuple-element.311, f32[2048]{0:T(1024)} %bitcast.51, f32[128]{0:T(128)S(1)} %add_rsqrt_fusion), kind=kOutput, calls=%fused_computation.5 | convolution fusion | flops 538181632 | bytes 5251584 | tf_op jit(solution)/shard_map/while/body/eval_jaxpr/cond/branch_1_fun/dot_general | solution.py:37
  69.0 1.3 fusion.9
  70.2 0.3 fusion.11
  71.0 0.8 fusion.24
  74.9 3.1 %fusion = bf16[128,2048]{1,0:T(8,128)(2,1)S(1)} fusion(bf16[1024,2048]{1,0:T(8,128)(2,1)} %get-tuple-element.322, bf16[128,2048]{1,0:T(8,128)(2,1)S(1)} %get-tuple-element.311, f32[128,1024]{1,0:T(8,128)S(1)} %pad.45, f32[128,1024]{1,0:T(8,128)S(1)} %pad.46), kind=kOutput, calls=%fused_computation.1 | convolution fusion | flops 537919488 | bytes 6291456 | tf_op jit(solution)/shard_map/while/body/eval_jaxpr/cond/branch_1_fun/dot_general | solution.py:64
  78.1 14.3 %collective-permute-done = bf16[128,2048]{1,0:T(8,128)(2,1)S(1)} collective-permute-done((bf16[128,2048]{1,0:T(8,128)(2,1)S(1)}, bf16[128,2048]{1,0:T(8,128)(2,1)S(1)}, u32[]{:S(2)}, u32[]{:S(2)}) %collective-permute-start) | collective-permute-done | bytes 524320 | tf_op jit(solution)/shard_map/while/body/eval_jaxpr/ppermute | solution.py:9
  92.5 14.2 %conditional.2 = (bf16[128,2048]{1,0:T(8,128)(2,1)S(1)}) conditional(s32[]{:T(128)} %convert_element_type.60, bf16[128,2048]{1,0:T(8,128)(2,1)S(1)} %get-tuple-element.499, (bf16[128,2048]{1,0:T(8,128)(2,1)S(1)}, f32[1,1024]{1,0:T(1,128)}, f32[1,2048]{1,0:T(1,128)}, bf16[2048,1024]{1,0:T(8,128)(2,1)}, f32[4,1024]{1,0:T(4,128)}, ...), branch_computations={%region_1.0_spmd, %region_2.3_spmd} | conditional | flops 1149344896 | bytes 37175976 | solution.py:107
  92.7 0.7 fusion.22
  93.4 0.9 fusion.31
  94.3 3.0 %fusion.1 = f32[128,1024]{1,0:T(8,128)S(1)} fusion(bf16[2048,1024]{1,0:T(8,128)(2,1)} %get-tuple-element.314, bf16[128,2048]{1,0:T(8,128)(2,1)S(1)} %get-tuple-element.311, f32[2048]{0:T(1024)} %bitcast.51, f32[128]{0:T(128)S(1)} %add_rsqrt_fusion), kind=kOutput, calls=%fused_computation.5 | convolution fusion | flops 538181632 | bytes 5251584 | tf_op jit(solution)/shard_map/while/body/eval_jaxpr/cond/branch_1_fun/dot_general | solution.py:37
  97.6 1.3 fusion.9
  98.9 0.3 fusion.11
  99.6 0.8 fusion.24
  103.6 3.1 %fusion = bf16[128,2048]{1,0:T(8,128)(2,1)S(1)} fusion(bf16[1024,2048]{1,0:T(8,128)(2,1)} %get-tuple-element.322, bf16[128,2048]{1,0:T(8,128)(2,1)S(1)} %get-tuple-element.311, f32[128,1024]{1,0:T(8,128)S(1)} %pad.45, f32[128,1024]{1,0:T(8,128)S(1)} %pad.46), kind=kOutput, calls=%fused_computation.1 | convolution fusion | flops 537919488 | bytes 6291456 | tf_op jit(solution)/shard_map/while/body/eval_jaxpr/cond/branch_1_fun/dot_general | solution.py:64
  106.7 13.5 %collective-permute-done = bf16[128,2048]{1,0:T(8,128)(2,1)S(1)} collective-permute-done((bf16[128,2048]{1,0:T(8,128)(2,1)S(1)}, bf16[128,2048]{1,0:T(8,128)(2,1)S(1)}, u32[]{:S(2)}, u32[]{:S(2)}) %collective-permute-start) | collective-permute-done | bytes 524320 | tf_op jit(solution)/shard_map/while/body/eval_jaxpr/ppermute | solution.py:9
  120.3 12.7 %collective-permute-start = (bf16[128,2048]{1,0:T(8,128)(2,1)S(1)}, bf16[128,2048]{1,0:T(8,128)(2,1)S(1)}, u32[]{:S(2)}, u32[]{:S(2)}) collective-permute-start(bf16[128,2048]{1,0:T(8,128)(2,1)S(1)} %get-tuple-element.530), channel_id=1, source_target_pairs={{0,8},{8,16},{16,24},{24,0},{1,9},{9,17},{17,25},{25,1},{2,10},{10... | collective-permute-start | bytes 1572872 | tf_op jit(solution)/shard_map/while/body/eval_jaxpr/ppermute | solution.py:9
  132.9 10.2 %collective-permute-done = bf16[128,2048]{1,0:T(8,128)(2,1)S(1)} collective-permute-done((bf16[128,2048]{1,0:T(8,128)(2,1)S(1)}, bf16[128,2048]{1,0:T(8,128)(2,1)S(1)}, u32[]{:S(2)}, u32[]{:S(2)}) %collective-permute-start) | collective-permute-done | bytes 524320 | tf_op jit(solution)/shard_map/while/body/eval_jaxpr/ppermute | solution.py:9
  143.2 1.8 collective-permute-start
  145.0 22.3 %collective-permute-done = bf16[128,2048]{1,0:T(8,128)(2,1)S(1)} collective-permute-done((bf16[128,2048]{1,0:T(8,128)(2,1)S(1)}, bf16[128,2048]{1,0:T(8,128)(2,1)S(1)}, u32[]{:S(2)}, u32[]{:S(2)}) %collective-permute-start) | collective-permute-done | bytes 524320 | tf_op jit(solution)/shard_map/while/body/eval_jaxpr/ppermute | solution.py:9
  167.4 0.8 collective-permute-start
  168.2 23.3 %collective-permute-done = bf16[128,2048]{1,0:T(8,128)(2,1)S(1)} collective-permute-done((bf16[128,2048]{1,0:T(8,128)(2,1)S(1)}, bf16[128,2048]{1,0:T(8,128)(2,1)S(1)}, u32[]{:S(2)}, u32[]{:S(2)}) %collective-permute-start) | collective-permute-done | bytes 524320 | tf_op jit(solution)/shard_map/while/body/eval_jaxpr/ppermute | solution.py:9
  191.6 11.3 %collective-permute-done = bf16[128,2048]{1,0:T(8,128)(2,1)S(1)} collective-permute-done((bf16[128,2048]{1,0:T(8,128)(2,1)S(1)}, bf16[128,2048]{1,0:T(8,128)(2,1)S(1)}, u32[]{:S(2)}, u32[]{:S(2)}) %collective-permute-start) | collective-permute-done | bytes 524320 | tf_op jit(solution)/shard_map/while/body/eval_jaxpr/ppermute | solution.py:9
  203.0 0.8 copy-done
  (374 shorter events, 14.9 us)
Async XLA Ops:
  4.0 4.8 %copy-start.1 = (f32[1,1024]{1,0:T(1,128)S(1)}, f32[1,1024]{1,0:T(1,128)}, u32[]{:S(2)}) copy-start(f32[1,1024]{1,0:T(1,128)} %get-tuple-element.312) | copy-start | bytes 12292 | tf_op jit(solution)/shard_map/while/body/eval_jaxpr/cond
  5.8 5.3 %copy-start.2 = (f32[1,1024]{1,0:T(1,128)S(1)}, f32[1,1024]{1,0:T(1,128)}, u32[]{:S(2)}) copy-start(f32[1,1024]{1,0:T(1,128)} %get-tuple-element.317) | copy-start | bytes 12292 | tf_op jit(solution)/shard_map/while/body/eval_jaxpr/cond
  5.8 5.3 %copy-start.3 = (f32[1,1024]{1,0:T(1,128)S(1)}, f32[1,1024]{1,0:T(1,128)}, u32[]{:S(2)}) copy-start(f32[1,1024]{1,0:T(1,128)} %get-tuple-element.321) | copy-start | bytes 12292 | tf_op jit(solution)/shard_map/while/body/eval_jaxpr/cond
  5.8 5.3 %copy-start.4 = (f32[1,128]{1,0:T(1,128)S(1)}, f32[1,128]{1,0:T(1,128)}, u32[]{:S(2)}) copy-start(f32[1,128]{1,0:T(1,128)} %get-tuple-element.319) | copy-start | bytes 1540 | tf_op jit(solution)/shard_map/while/body/eval_jaxpr/cond
  18.1 16.2 %collective-permute-start = (bf16[128,2048]{1,0:T(8,128)(2,1)S(1)}, bf16[128,2048]{1,0:T(8,128)(2,1)S(1)}, u32[]{:S(2)}, u32[]{:S(2)}) collective-permute-start(bf16[128,2048]{1,0:T(8,128)(2,1)S(1)} %get-tuple-element.530), channel_id=1, source_target_pairs={{0,8},{8,16},{16,24},{24,0},{1,9},{9,17},{17,25},{25,1},{2,10},{10... | collective-permute-start | bytes 1572872 | tf_op jit(solution)/shard_map/while/body/eval_jaxpr/ppermute | solution.py:9
  34.3 4.8 %copy-start.1 = (f32[1,1024]{1,0:T(1,128)S(1)}, f32[1,1024]{1,0:T(1,128)}, u32[]{:S(2)}) copy-start(f32[1,1024]{1,0:T(1,128)} %get-tuple-element.312) | copy-start | bytes 12292 | tf_op jit(solution)/shard_map/while/body/eval_jaxpr/cond
  36.2 5.3 %copy-start.2 = (f32[1,1024]{1,0:T(1,128)S(1)}, f32[1,1024]{1,0:T(1,128)}, u32[]{:S(2)}) copy-start(f32[1,1024]{1,0:T(1,128)} %get-tuple-element.317) | copy-start | bytes 12292 | tf_op jit(solution)/shard_map/while/body/eval_jaxpr/cond
  36.2 5.3 %copy-start.3 = (f32[1,1024]{1,0:T(1,128)S(1)}, f32[1,1024]{1,0:T(1,128)}, u32[]{:S(2)}) copy-start(f32[1,1024]{1,0:T(1,128)} %get-tuple-element.321) | copy-start | bytes 12292 | tf_op jit(solution)/shard_map/while/body/eval_jaxpr/cond
  36.2 5.3 %copy-start.4 = (f32[1,128]{1,0:T(1,128)S(1)}, f32[1,128]{1,0:T(1,128)}, u32[]{:S(2)}) copy-start(f32[1,128]{1,0:T(1,128)} %get-tuple-element.319) | copy-start | bytes 1540 | tf_op jit(solution)/shard_map/while/body/eval_jaxpr/cond
  48.5 15.3 %collective-permute-start = (bf16[128,2048]{1,0:T(8,128)(2,1)S(1)}, bf16[128,2048]{1,0:T(8,128)(2,1)S(1)}, u32[]{:S(2)}, u32[]{:S(2)}) collective-permute-start(bf16[128,2048]{1,0:T(8,128)(2,1)S(1)} %get-tuple-element.530), channel_id=1, source_target_pairs={{0,8},{8,16},{16,24},{24,0},{1,9},{9,17},{17,25},{25,1},{2,10},{10... | collective-permute-start | bytes 1572872 | tf_op jit(solution)/shard_map/while/body/eval_jaxpr/ppermute | solution.py:9
  63.9 4.8 %copy-start.1 = (f32[1,1024]{1,0:T(1,128)S(1)}, f32[1,1024]{1,0:T(1,128)}, u32[]{:S(2)}) copy-start(f32[1,1024]{1,0:T(1,128)} %get-tuple-element.312) | copy-start | bytes 12292 | tf_op jit(solution)/shard_map/while/body/eval_jaxpr/cond
  65.7 5.3 %copy-start.2 = (f32[1,1024]{1,0:T(1,128)S(1)}, f32[1,1024]{1,0:T(1,128)}, u32[]{:S(2)}) copy-start(f32[1,1024]{1,0:T(1,128)} %get-tuple-element.317) | copy-start | bytes 12292 | tf_op jit(solution)/shard_map/while/body/eval_jaxpr/cond
  65.7 5.3 %copy-start.3 = (f32[1,1024]{1,0:T(1,128)S(1)}, f32[1,1024]{1,0:T(1,128)}, u32[]{:S(2)}) copy-start(f32[1,1024]{1,0:T(1,128)} %get-tuple-element.321) | copy-start | bytes 12292 | tf_op jit(solution)/shard_map/while/body/eval_jaxpr/cond
  65.7 5.3 %copy-start.4 = (f32[1,128]{1,0:T(1,128)S(1)}, f32[1,128]{1,0:T(1,128)}, u32[]{:S(2)}) copy-start(f32[1,128]{1,0:T(1,128)} %get-tuple-element.319) | copy-start | bytes 1540 | tf_op jit(solution)/shard_map/while/body/eval_jaxpr/cond
  78.0 14.4 %collective-permute-start = (bf16[128,2048]{1,0:T(8,128)(2,1)S(1)}, bf16[128,2048]{1,0:T(8,128)(2,1)S(1)}, u32[]{:S(2)}, u32[]{:S(2)}) collective-permute-start(bf16[128,2048]{1,0:T(8,128)(2,1)S(1)} %get-tuple-element.530), channel_id=1, source_target_pairs={{0,8},{8,16},{16,24},{24,0},{1,9},{9,17},{17,25},{25,1},{2,10},{10... | collective-permute-start | bytes 1572872 | tf_op jit(solution)/shard_map/while/body/eval_jaxpr/ppermute | solution.py:9
  92.5 4.8 %copy-start.1 = (f32[1,1024]{1,0:T(1,128)S(1)}, f32[1,1024]{1,0:T(1,128)}, u32[]{:S(2)}) copy-start(f32[1,1024]{1,0:T(1,128)} %get-tuple-element.312) | copy-start | bytes 12292 | tf_op jit(solution)/shard_map/while/body/eval_jaxpr/cond
  94.3 5.3 %copy-start.2 = (f32[1,1024]{1,0:T(1,128)S(1)}, f32[1,1024]{1,0:T(1,128)}, u32[]{:S(2)}) copy-start(f32[1,1024]{1,0:T(1,128)} %get-tuple-element.317) | copy-start | bytes 12292 | tf_op jit(solution)/shard_map/while/body/eval_jaxpr/cond
  94.3 5.3 %copy-start.3 = (f32[1,1024]{1,0:T(1,128)S(1)}, f32[1,1024]{1,0:T(1,128)}, u32[]{:S(2)}) copy-start(f32[1,1024]{1,0:T(1,128)} %get-tuple-element.321) | copy-start | bytes 12292 | tf_op jit(solution)/shard_map/while/body/eval_jaxpr/cond
  94.3 5.3 %copy-start.4 = (f32[1,128]{1,0:T(1,128)S(1)}, f32[1,128]{1,0:T(1,128)}, u32[]{:S(2)}) copy-start(f32[1,128]{1,0:T(1,128)} %get-tuple-element.319) | copy-start | bytes 1540 | tf_op jit(solution)/shard_map/while/body/eval_jaxpr/cond
  106.6 13.5 %collective-permute-start = (bf16[128,2048]{1,0:T(8,128)(2,1)S(1)}, bf16[128,2048]{1,0:T(8,128)(2,1)S(1)}, u32[]{:S(2)}, u32[]{:S(2)}) collective-permute-start(bf16[128,2048]{1,0:T(8,128)(2,1)S(1)} %get-tuple-element.530), channel_id=1, source_target_pairs={{0,8},{8,16},{16,24},{24,0},{1,9},{9,17},{17,25},{25,1},{2,10},{10... | collective-permute-start | bytes 1572872 | tf_op jit(solution)/shard_map/while/body/eval_jaxpr/ppermute | solution.py:9
  120.3 22.8 %collective-permute-start = (bf16[128,2048]{1,0:T(8,128)(2,1)S(1)}, bf16[128,2048]{1,0:T(8,128)(2,1)S(1)}, u32[]{:S(2)}, u32[]{:S(2)}) collective-permute-start(bf16[128,2048]{1,0:T(8,128)(2,1)S(1)} %get-tuple-element.530), channel_id=1, source_target_pairs={{0,8},{8,16},{16,24},{24,0},{1,9},{9,17},{17,25},{25,1},{2,10},{10... | collective-permute-start | bytes 1572872 | tf_op jit(solution)/shard_map/while/body/eval_jaxpr/ppermute | solution.py:9
  143.2 24.2 %collective-permute-start = (bf16[128,2048]{1,0:T(8,128)(2,1)S(1)}, bf16[128,2048]{1,0:T(8,128)(2,1)S(1)}, u32[]{:S(2)}, u32[]{:S(2)}) collective-permute-start(bf16[128,2048]{1,0:T(8,128)(2,1)S(1)} %get-tuple-element.530), channel_id=1, source_target_pairs={{0,8},{8,16},{16,24},{24,0},{1,9},{9,17},{17,25},{25,1},{2,10},{10... | collective-permute-start | bytes 1572872 | tf_op jit(solution)/shard_map/while/body/eval_jaxpr/ppermute | solution.py:9
  167.4 24.1 %collective-permute-start = (bf16[128,2048]{1,0:T(8,128)(2,1)S(1)}, bf16[128,2048]{1,0:T(8,128)(2,1)S(1)}, u32[]{:S(2)}, u32[]{:S(2)}) collective-permute-start(bf16[128,2048]{1,0:T(8,128)(2,1)S(1)} %get-tuple-element.530), channel_id=1, source_target_pairs={{0,8},{8,16},{16,24},{24,0},{1,9},{9,17},{17,25},{25,1},{2,10},{10... | collective-permute-start | bytes 1572872 | tf_op jit(solution)/shard_map/while/body/eval_jaxpr/ppermute | solution.py:9
  191.6 11.4 %collective-permute-start = (bf16[128,2048]{1,0:T(8,128)(2,1)S(1)}, bf16[128,2048]{1,0:T(8,128)(2,1)S(1)}, u32[]{:S(2)}, u32[]{:S(2)}) collective-permute-start(bf16[128,2048]{1,0:T(8,128)(2,1)S(1)} %get-tuple-element.530), channel_id=1, source_target_pairs={{0,8},{8,16},{16,24},{24,0},{1,9},{9,17},{17,25},{25,1},{2,10},{10... | collective-permute-start | bytes 1572872 | tf_op jit(solution)/shard_map/while/body/eval_jaxpr/ppermute | solution.py:9
  203.0 0.8 copy-start
where the time goes:
time: 205 us; the launch traced here: 204 us
  waiting for transfers between devices  126 us (61%)
  matrix products  30.4 us (15%)
  local copies, waits for them, and re-layouts  19.1 us (9%)
  starting transfers between devices  15.6 us (8%)
  other arithmetic  9.96 us (5%)
  loops' own time  2.54 us (1%)
    ppermute x8, waiting for transfers between devices, from_behind(): lax.ppermute(value, axis, [(i, (i + by) % devices) for i in range(devices)])  126 us
    ppermute x8, starting transfers between devices, from_behind(): lax.ppermute(value, axis, [(i, (i + by) % devices) for i in range(devices)])  15.6 us
    dot_general x4, matrix products, one_layer(): jnp.dot(states, output_projected, preferred_element_type=jnp.float32)  12.3 us
    dot_general x4, matrix products, one_layer(): jnp.dot(normed, input_projected, preferred_element_type=jnp.float32)  11.9 us
    slice x156, local copies, waits for them, and re-layouts, one_layer(): lax.associative_scan(combine_pair, (decay, update), axis=0)[1]  7.38 us
    dot_general x4, matrix products, one_layer(): jnp.einsum('ngi,gij->ngj', grouped, injection_weight, preferred_element_t...  5.02 us
    unnamed x5, local copies, waits for them, and re-layouts  4.74 us
  transfers between devices with their start and end apart: 8, of which 8 were waited for; matrix products, arithmetic and copies ran while one was open for 0% of the time, Pallas kernels for 0%

commit v1 on v0

v1 whole, which is shorter than its diff:
```python
import functools

import jax
import jax.numpy as jnp
from jax import lax
from jax.experimental import pallas as pl
from jax.experimental.pallas import tpu as pltpu
from jax.sharding import PartitionSpec as P

MESH = pl.DeviceIdType.MESH
CHUNKS = 4
GROUP = 8
LANES = 128


def one_minus_exp(y):
    series = -y * (1.0 + y * (0.5 + y * (1.0 / 6.0 + y * (1.0 / 24.0 + y * (1.0 / 120.0)))))
    return jnp.where(y > -0.25, series, 1.0 - jnp.exp(y))


def kernel(
    stages,
    chunks,
    tokens,
    scale,
    w_in_hbm,
    taps,
    tap_bias,
    gr_hbm,
    bias_r,
    gi_hbm,
    bias_i,
    decay_setting,
    spike,
    w_out_hbm,
    out,
    x_in,
    y_out,
    landed,
    w_in,
    w_out,
    gates,
    tails,
    carries,
    rates,
    spikes,
    states,
    in_sem,
    send_sem,
    tok_sem,
    res_sem,
    w_sem,
    out_sem,
):
    me = lax.axis_index("pp")
    last = stages - 1
    length, width = tokens.shape
    rows = length // chunks
    channels = w_in.shape[1]
    blocks = gates.shape[0]
    ntaps = taps.shape[0]

    def chunk_rows(c):
        return pl.ds(pl.multiple_of(c * rows, rows), rows)

    def token_copy(c):
        return pltpu.make_async_remote_copy(
            src_ref=tokens.at[chunk_rows(c)],
            dst_ref=x_in.at[me, c],
            send_sem=tok_sem.at[c],
            recv_sem=in_sem.at[me, c],
            device_id={"pp": 0},
            device_id_type=MESH,
        )

    def forward_copy(m, c):
        return pltpu.make_async_remote_copy(
            src_ref=y_out.at[m, c],
            dst_ref=x_in.at[m, c],
            send_sem=send_sem.at[m, c],
            recv_sem=in_sem.at[m, c],
            device_id={"pp": me + 1},
            device_id_type=MESH,
        )

    def home_copy(m, c):
        return pltpu.make_async_remote_copy(
            src_ref=y_out.at[m, c],
            dst_ref=landed.at[c],
            send_sem=send_sem.at[m, c],
            recv_sem=res_sem.at[c],
            device_id={"pp": m},
            device_id_type=MESH,
        )

    weight_copies = [
        pltpu.make_async_copy(w_in_hbm, w_in, w_sem.at[0]),
        pltpu.make_async_copy(gr_hbm, gates.at[:, :, pl.ds(0, LANES)], w_sem.at[1]),
        pltpu.make_async_copy(gi_hbm, gates.at[:, :, pl.ds(LANES, LANES)], w_sem.at[2]),
        pltpu.make_async_copy(w_out_hbm, w_out, w_sem.at[3]),
    ]

    barrier = pltpu.get_barrier_semaphore()
    for step in range(1, stages):
        pl.semaphore_signal(
            barrier, inc=1, device_id={"pp": lax.rem(me + step, stages)}, device_id_type=MESH
        )

    @pl.when(me == 0)
    def _():
        for c in range(chunks):
            pltpu.make_async_copy(tokens.at[chunk_rows(c)], x_in.at[0, c], in_sem.at[0, c]).start()

    for copy in weight_copies:
        copy.start()
    rates[...] = -8.0 * (
        jnp.maximum(-decay_setting[...], 0.0)
        + jnp.log1p(jnp.exp(-jnp.abs(decay_setting[...])))
    )
    spikes[...] = jnp.broadcast_to(spike[...], (LANES, length)).T
    tails[...] = jnp.zeros_like(tails)
    carries[...] = jnp.zeros_like(carries)
    pl.semaphore_wait(barrier, stages - 1)

    @pl.when(me > 0)
    def _():
        for c in range(chunks):
            token_copy(c).start()

    for copy in weight_copies:
        copy.wait()

    def layer(m, c):
        hidden = x_in[m, c].astype(jnp.float32)
        squares = jnp.mean(hidden * hidden, axis=-1, keepdims=True)
        normed = (hidden * lax.rsqrt(squares + 1e-6) * scale[...]).astype(jnp.bfloat16)
        row_in_group = lax.broadcasted_iota(jnp.int32, (rows // GROUP, GROUP, LANES), 1)
        spiked = spikes[chunk_rows(c), :]
        pair = 2 * LANES
        for two in range(channels // pair):
            wide = slice(two * pair, (two + 1) * pair)
            mixed = jnp.dot(normed, w_in[:, wide], preferred_element_type=jnp.float32)
            mixed = mixed.astype(jnp.bfloat16).astype(jnp.float32)
            padded = jnp.concatenate([tails[m, :, wide], mixed], axis=0)
            tails[m, :, wide] = mixed[rows - GROUP :]
            conv = tap_bias[:, wide]
            for k in range(ntaps):
                start = GROUP - (ntaps - 1) + k
                conv = conv + padded[start : start + rows] * taps[k : k + 1, wide]
            conv = conv.astype(jnp.bfloat16)
            for half in range(2):
                g = 2 * two + half
                lanes = slice(g * LANES, (g + 1) * LANES)
                mine = conv[:, half * LANES : (half + 1) * LANES]
                z = jnp.dot(mine, gates[g], preferred_element_type=jnp.float32)
                recall = jax.nn.sigmoid(z[:, :LANES] + bias_r[:, lanes])
                inject = jax.nn.sigmoid(z[:, LANES:] + bias_i[:, lanes])
                log_decay = recall * rates[:, lanes] + spiked
                a = jnp.exp(log_decay)
                u = jnp.sqrt(one_minus_exp(2.0 * log_decay)) * inject * mine.astype(jnp.float32)
                a = a.reshape(rows // GROUP, GROUP, LANES)
                u = u.reshape(rows // GROUP, GROUP, LANES)
                for by in (1, 2, 4):
                    inside = row_in_group >= by
                    u = u + a * jnp.where(inside, pltpu.roll(u, by, 1), 0.0)
                    a = a * jnp.where(inside, pltpu.roll(a, by, 1), 1.0)
                carry = carries[m, :, lanes]
                parts = []
                for i in range(rows // GROUP):
                    h = a[i] * carry + u[i]
                    parts.append(h)
                    carry = jnp.broadcast_to(h[GROUP - 1 :], (GROUP, LANES))
                carries[m, :, lanes] = carry
                states[:, lanes] = jnp.concatenate(parts, axis=0).astype(jnp.bfloat16)
        projected = jnp.dot(states[...], w_out[...], preferred_element_type=jnp.float32)
        y_out[m, c] = (x_in[m, c].astype(jnp.float32) + projected).astype(jnp.bfloat16)

    def advance(i, _):
        j = jnp.maximum(i - chunks, 0)
        others = max(stages - 1, 1)
        first = i < chunks
        m = jnp.where(first, 0, 1 + j % others)
        c = jnp.where(first, i, j // others)
        pltpu.make_async_copy(x_in.at[m, c], x_in.at[m, c], in_sem.at[m, c]).wait()
        layer(m, c)

        @pl.when(me < last)
        def _():
            forward_copy(m, c).start()

        @pl.when((me == last) & (m < last))
        def _():
            home_copy(m, c).start()

        return 0

    lax.fori_loop(0, stages * chunks, advance, 0)

    def final_copy(source, c):
        return pltpu.make_async_copy(source, out.at[chunk_rows(c)], out_sem.at[c])

    @pl.when(me == last)
    def _():
        for c in range(chunks):
            final_copy(y_out.at[last, c], c).start()

    @pl.when(me < last)
    def _():
        for c in range(chunks):
            pltpu.make_async_copy(landed.at[c], landed.at[c], res_sem.at[c]).wait()
            final_copy(landed.at[c], c).start()

    @pl.when(me > 0)
    def _():
        for c in range(chunks):
            token_copy(c).wait_send()

    def drain(i, _):
        m = i // chunks
        c = i % chunks

        @pl.when(me < last)
        def _():
            forward_copy(m, c).wait_send()

        @pl.when((me == last) & (m < last))
        def _():
            home_copy(m, c).wait_send()

        return 0

    lax.fori_loop(0, stages * chunks, drain, 0)
    for c in range(chunks):
        final_copy(landed.at[c], c).wait()


def solution(mesh):
    stages = mesh.shape["pp"]

    def local(
        tokens, norm, w_in, taps, tap_bias, gr, br, gi, bi, decay_setting, spike, w_out
    ):
        length, width = tokens.shape[2:]
        channels = w_in.shape[2]
        blocks, wide = gr.shape[1:3]
        rows = length // CHUNKS
        vmem = pl.BlockSpec(memory_space=pltpu.VMEM)
        anywhere = pl.BlockSpec(memory_space=pl.ANY)
        result = pl.pallas_call(
            functools.partial(kernel, stages, CHUNKS),
            out_shape=jax.ShapeDtypeStruct((length, width), jnp.bfloat16),
            in_specs=[
                anywhere, vmem, anywhere, vmem, vmem, anywhere, vmem, anywhere, vmem, vmem, vmem,
                anywhere,
            ],
            out_specs=anywhere,
            scratch_shapes=[
                pltpu.VMEM((stages, CHUNKS, rows, width), jnp.bfloat16),
                pltpu.VMEM((stages, CHUNKS, rows, width), jnp.bfloat16),
                pltpu.VMEM((CHUNKS, rows, width), jnp.bfloat16),
                pltpu.VMEM((width, channels), jnp.bfloat16),
                pltpu.VMEM((channels, width), jnp.bfloat16),
                pltpu.VMEM((blocks, wide, 2 * wide), jnp.bfloat16),
                pltpu.VMEM((stages, GROUP, channels), jnp.float32),
                pltpu.VMEM((stages, GROUP, channels), jnp.float32),
                pltpu.VMEM((1, channels), jnp.float32),
                pltpu.VMEM((length, LANES), jnp.float32),
                pltpu.VMEM((rows, channels), jnp.bfloat16),
                pltpu.SemaphoreType.DMA((stages, CHUNKS)),
                pltpu.SemaphoreType.DMA((stages, CHUNKS)),
                pltpu.SemaphoreType.DMA((CHUNKS,)),
                pltpu.SemaphoreType.DMA((CHUNKS,)),
                pltpu.SemaphoreType.DMA((4,)),
                pltpu.SemaphoreType.DMA((CHUNKS,)),
            ],
            compiler_params=pltpu.CompilerParams(
                collective_id=0, has_side_effects=True, vmem_limit_bytes=60 * 1024 * 1024
            ),
        )(
            tokens[0, 0], norm, w_in[0], taps[0], tap_bias, gr[0], br, gi[0], bi, decay_setting,
            spike, w_out[0],
        )
        return result[None, None]

    placed = (
        P("pp", ("fs", "tp"), None, None),
        P("pp", None),
        P("pp", None, None),
        P("pp", None, None),
        P("pp", None),
        P("pp", None, None, None),
        P("pp", None),
        P("pp", None, None, None),
        P("pp", None),
        P("pp", None),
        P("pp", None),
        P("pp", None, None),
    )
    return jax.shard_map(
        local,
        mesh=mesh,
        in_specs=placed,
        out_specs=P("pp", ("fs", "tp"), None, None),
        check_vma=False,
    )
```

time: 205 us -> 101 us (0.49)
  the two profiles are of different devices: /device:TPU:0 before, /device:TPU:16 now
where the time goes in v1:
time: 101 us
  Pallas kernels  99.3 us (98%)
  local copies, waits for them, and re-layouts  1.88 us (2%)
    pallas_call x1, Pallas kernels, local(): pl.pallas_call(functools.partial(kernel, stages, CHUNKS), out_shape=jax.S...  99.3 us

profile of v1, /device:TPU:16, one launch (start us, length us, event | category | flops | bytes accessed | tf_op | source)
XLA Modules:
  0.0 101.2 jit_solution(12157616627017323583)
XLA Ops:
  0.0 99.3 %shard_map.118 = bf16[128,2048]{1,0:T(8,128)(2,1)} custom-call(bf16[128,2048]{1,0:T(8,128)(2,1)} %bitcast.10, f32[1,2048]{1,0:T(1,128)} %scale.1, bf16[2048,1024]{1,0:T(8,128)(2,1)} %bitcast.7, f32[4,1024]{1,0:T(4,128)} %bitcast.13, f32[1,1024]{1,0:T(1,128)} %tap_bias.1, bf16[8,128,128]{2,1,0:T(8,128)(2,1)} %bitcast.11, f32[1,1024]{1,0:T(1,128)} %bias_r.1, ...), custom_call_target="tpu_custom_call" | custom-call | tf_op jit(solution)/shard_map/pallas_call | solution.py:249
  99.3 1.9 %copy.14 = bf16[1,1,128,2048]{3,2,1,0:T(8,128)(2,1)} copy(bf16[1,1,128,2048]{3,2,1,0:T(8,128)(2,1)} %bitcast.9) | data formatting | bytes 1048576

commit v2 on v1

--- a/solution.py
+++ b/solution.py
@@ -9,6 +9,8 @@
 
 MESH = pl.DeviceIdType.MESH
 CHUNKS = 4
+GO_CHUNK = CHUNKS - 1
+DEFER = CHUNKS
 GROUP = 8
 LANES = 128
 
@@ -51,6 +53,7 @@
     res_sem,
     w_sem,
     out_sem,
+    go_sem,
 ):
     me = lax.axis_index("pp")
     last = stages - 1
@@ -122,7 +125,7 @@
     carries[...] = jnp.zeros_like(carries)
     pl.semaphore_wait(barrier, stages - 1)
 
-    @pl.when(me > 0)
+    @pl.when(me == 1)
     def _():
         for c in range(chunks):
             token_copy(c).start()
@@ -176,11 +179,20 @@
         y_out[m, c] = (x_in[m, c].astype(jnp.float32) + projected).astype(jnp.bfloat16)
 
     def advance(i, _):
-        j = jnp.maximum(i - chunks, 0)
-        others = max(stages - 1, 1)
-        first = i < chunks
-        m = jnp.where(first, 0, 1 + j % others)
-        c = jnp.where(first, i, j // others)
+        m = i // chunks
+        c = i % chunks
+
+        @pl.when((me > 1) & (i == jnp.maximum(me - 2, 0)))
+        def _():
+            pl.semaphore_wait(go_sem, 1)
+            for q in range(chunks):
+                token_copy(q).start()
+
+        @pl.when((me > 0) & (me < last) & (i == me + 0))
+        def _():
+            token_copy(GO_CHUNK).wait_send()
+            pl.semaphore_signal(go_sem, inc=1, device_id={"pp": me + 1}, device_id_type=MESH)
+
         pltpu.make_async_copy(x_in.at[m, c], x_in.at[m, c], in_sem.at[m, c]).wait()
         layer(m, c)
 
@@ -188,9 +200,13 @@
         def _():
             forward_copy(m, c).start()
 
-        @pl.when((me == last) & (m < last))
+        @pl.when((me == last) & (m < last) & (m > 0))
         def _():
             home_copy(m, c).start()
+
+        @pl.when((me == last) & (i >= DEFER) & (i < DEFER + chunks))
+        def _():
+            home_copy(0, i - DEFER).start()
 
         return 0
 
@@ -213,7 +229,12 @@
     @pl.when(me > 0)
     def _():
         for c in range(chunks):
-            token_copy(c).wait_send()
+            if c != GO_CHUNK:
+                token_copy(c).wait_send()
+
+    @pl.when(me == last)
+    def _():
+        token_copy(GO_CHUNK).wait_send()
 
     def drain(i, _):
         m = i // chunks
@@ -272,6 +293,7 @@
                 pltpu.SemaphoreType.DMA((CHUNKS,)),
                 pltpu.SemaphoreType.DMA((4,)),
                 pltpu.SemaphoreType.DMA((CHUNKS,)),
+                pltpu.SemaphoreType.REGULAR,
             ],
             compiler_params=pltpu.CompilerParams(
                 collective_id=0, has_side_effects=True, vmem_limit_bytes=60 * 1024 * 1024

time: 101 us -> 78.3 us (0.78)
  Pallas kernels: 99.3 us -> 76.2 us
    pallas_call x1, Pallas kernels: 99.3 us -> 76.2 us  [local(): pl.pallas_call(functools.partial(kernel, stages, CHUNKS), out_shape=jax.S...]
where the time goes in v2:
time: 78.3 us; the launch traced here: 78.1 us
  Pallas kernels  76.2 us (97%)
  local copies, waits for them, and re-layouts  1.88 us (2%)
    pallas_call x1, Pallas kernels, local(): pl.pallas_call(functools.partial(kernel, stages, CHUNKS), out_shape=jax.S...  76.2 us
    unnamed x1, local copies, waits for them, and re-layouts  1.88 us

profile of v2, /device:TPU:16, one launch (start us, length us, event | category | flops | bytes accessed | tf_op | source)
XLA Modules:
  0.0 78.1 jit_solution(13964635642253319722)
XLA Ops:
  0.0 76.2 %shard_map.118 = bf16[128,2048]{1,0:T(8,128)(2,1)} custom-call(bf16[128,2048]{1,0:T(8,128)(2,1)} %bitcast.10, f32[1,2048]{1,0:T(1,128)} %scale.1, bf16[2048,1024]{1,0:T(8,128)(2,1)} %bitcast.7, f32[4,1024]{1,0:T(4,128)} %bitcast.13, f32[1,1024]{1,0:T(1,128)} %tap_bias.1, bf16[8,128,128]{2,1,0:T(8,128)(2,1)} %bitcast.11, f32[1,1024]{1,0:T(1,128)} %bias_r.1, ...), custom_call_target="tpu_custom_call" | custom-call | tf_op jit(solution)/shard_map/pallas_call | solution.py:270
  76.2 1.9 %copy.14 = bf16[1,1,128,2048]{3,2,1,0:T(8,128)(2,1)} copy(bf16[1,1,128,2048]{3,2,1,0:T(8,128)(2,1)} %bitcast.9) | data formatting | bytes 1048576
